TPU v7x, 32 devices: a whole 2x2x4 slice. The times are simulated.
32 devices in a mesh: sp: 8 (over z, x), tp: 4 (over y, core).
Axes of the slice: x: 2, y: 2, z: 4, core: 2. Of those that a mesh axis runs over, the one named last changes fastest.
Arguments:
- queries: bfloat16 [4096, 512], P('sp', 'tp'), may hold values from -16 to 16
- key_heads: bfloat16 [4096, 512], P('sp', 'tp'), may hold values from -16 to 16
- value_heads: bfloat16 [4096, 512], P('sp', 'tp'), may hold values from -6 to 6
- head_gain: float32 [512], P('tp'), may hold values from 0.1 to 1.9
- residual: bfloat16 [4096, 2048], P(('sp', 'tp')), may hold values from -6 to 6
- out_weight: bfloat16 [512, 2048], replicated, may hold values from -0.25 to 0.25
- norm_gain: float32 [2048], replicated, may hold values from 0.1 to 1.9
- shared_gate: bfloat16 [2048, 512], replicated, may hold values from -0.125 to 0.125
- shared_up: bfloat16 [2048, 512], replicated, may hold values from -0.125 to 0.125
- shared_down: bfloat16 [512, 2048], replicated, may hold values from -0.25 to 0.25
- expert_gate: bfloat16 [64, 2048, 512], P(('sp', 'tp')), may hold values from -0.125 to 0.125
- expert_up: bfloat16 [64, 2048, 512], P(('sp', 'tp')), may hold values from -0.125 to 0.125
- expert_down: bfloat16 [64, 512, 2048], P(('sp', 'tp')), may hold values from -0.25 to 0.25
- routed_experts: int32 [4096, 4], P(('sp', 'tp')), may hold values from 0 to 63, all different within a row; in each aligned block of 128 rows (0 to 127, 128 to 255, ...) at most 12 rows name the same one
- route_weights: float32 [4096, 4], P(('sp', 'tp')), may hold values from 0.1 to 1.5
Outputs:
- layer_output: bfloat16 [4096, 2048], P(('sp', 'tp'))
Inputs may be any that keep to these rules, and one draw needn't show every extreme that they name: `routed_experts`: each row names 4 different experts. Within the rows of one device (128 consecutive rows, aligned) no expert is named more than 12 times, and in every draw some expert is named exactly 12 times in some device's rows.
All inputs are finite; a program needn't handle non-finite values.
Results may differ from a plain program's by a relative error of at most 0.014.
Values may be sent and summed in bfloat16 or wider, within the bound.
A program may use at most 128 MiB of HBM per device.

v0:
```python
import math
import jax
import jax.numpy as jnp
from jax import lax
from jax.sharding import PartitionSpec as P

HEAD_DIM = 64
EPSILON = 1e-06


def block_terms(query_block, key_block, value_block, query_start, key_start):
    scale = 1.0 / math.sqrt(HEAD_DIM)
    scores = (
        jnp.einsum("qhd,khd->hqk", query_block, key_block, preferred_element_type=jnp.float32)
        * scale
    )
    query_places = query_start + lax.iota(jnp.int32, query_block.shape[0])
    key_places = key_start + lax.iota(jnp.int32, key_block.shape[0])
    earlier = (key_places[None, :] < query_places[:, None])[None]
    stay_log = jnp.where(earlier, jax.nn.log_sigmoid(-scores), 0.0)
    after_log = lax.cumsum(stay_log, axis=2, reverse=True) - stay_log
    weights = jnp.where(earlier, jnp.exp(jax.nn.log_sigmoid(scores) + after_log), 0.0).astype(
        jnp.bfloat16
    )
    partial_out = jnp.einsum(
        "hqk,khd->qhd", weights, value_block, preferred_element_type=jnp.float32
    )
    block_total = jnp.transpose(jnp.sum(stay_log, axis=2))
    return (block_total, partial_out)


def head_norm(mixed, head_gain):
    inverse = lax.rsqrt(jnp.mean(mixed * mixed, axis=2, keepdims=True) + EPSILON)
    normed = mixed * inverse * head_gain.reshape(mixed.shape[1], mixed.shape[2])
    return normed.reshape(mixed.shape[0], -1).astype(jnp.bfloat16)


def stick_breaking(queries, key_heads, value_heads):
    seq_count = queries.shape[0]
    head_count = queries.shape[1] // HEAD_DIM
    shard_count = lax.axis_size("sp")
    shard_place = lax.axis_index("sp")
    query_width = 512
    query_blocks = queries.reshape(seq_count // query_width, query_width, head_count, HEAD_DIM)
    block_starts = shard_place * seq_count + query_width * jnp.arange(
        seq_count // query_width, dtype=jnp.int32
    )

    def shard_terms(key_block, value_block, key_start):

        def one_block(inputs):
            query_block, query_start = inputs
            return block_terms(query_block, key_block, value_block, query_start, key_start)

        totals, partials = lax.map(one_block, (query_blocks, block_starts))
        return (
            totals.reshape(seq_count, head_count),
            partials.reshape(seq_count, head_count, HEAD_DIM),
        )

    initial = (
        jnp.zeros((shard_count, seq_count, head_count), jnp.float32),
        jnp.zeros((shard_count, seq_count, head_count, HEAD_DIM), jnp.float32),
    )
    key_piece = lax.all_gather(key_heads, "sp", axis=0, tiled=True).reshape(
        -1, seq_count, head_count, HEAD_DIM
    )
    value_piece = lax.all_gather(value_heads, "sp", axis=0, tiled=True).reshape(
        -1, seq_count, head_count, HEAD_DIM
    )

    def add_one(shard_step, state):
        total_store, partial_store = state
        key_block = lax.dynamic_index_in_dim(key_piece, shard_step, 0, keepdims=False)
        value_block = lax.dynamic_index_in_dim(value_piece, shard_step, 0, keepdims=False)

        def compute(unused):
            return shard_terms(key_block, value_block, shard_step * seq_count)

        def nothing(unused):
            return (
                jnp.zeros((seq_count, head_count), jnp.float32),
                jnp.zeros((seq_count, head_count, HEAD_DIM), jnp.float32),
            )

        totals, partials = lax.cond(shard_step <= shard_place, compute, nothing, 0)
        total_store = lax.dynamic_update_index_in_dim(total_store, totals, shard_step, 0)
        partial_store = lax.dynamic_update_index_in_dim(partial_store, partials, shard_step, 0)
        return (total_store, partial_store)

    totals, partials = lax.fori_loop(0, key_piece.shape[0], add_one, initial)
    later = lax.cumsum(totals, axis=0, reverse=True) - totals
    return jnp.sum(jnp.exp(later)[..., None] * partials, axis=0)


def routed_sum(expert_input, expert_gate, expert_up, expert_down, routed_experts, route_weights):
    row_count, pick_count = routed_experts.shape
    local_experts = expert_gate.shape[0]
    model_width = expert_input.shape[1]
    sp_count = lax.axis_size("sp")
    tp_count = lax.axis_size("tp")
    device_count = sp_count * tp_count
    expert_count = local_experts * device_count
    capacity = max(2, 3 * row_count * pick_count // (2 * expert_count))
    flat_experts = routed_experts.reshape(-1)
    expert_table = (
        flat_experts[:, None] == jnp.arange(expert_count, dtype=jnp.int32)[None, :]
    ).astype(jnp.int32)
    ranking = jnp.sum(jnp.cumsum(expert_table, axis=0) * expert_table, axis=1) - 1
    holder = flat_experts // local_experts
    resident = flat_experts % local_experts
    slot_index = (resident * device_count + holder) * capacity + ranking
    placement = (
        slot_index[:, None] == jnp.arange(expert_count * capacity, dtype=jnp.int32)[None, :]
    ).astype(jnp.bfloat16)
    token_place = jnp.sum(placement.reshape(row_count, pick_count, -1), axis=1)
    outgoing = jnp.einsum(
        "rs,rd->sd", token_place, expert_input, preferred_element_type=jnp.float32
    ).astype(jnp.bfloat16)
    outgoing = outgoing.reshape(local_experts, device_count, capacity, model_width)
    arrived = lax.all_to_all(outgoing, ("sp", "tp"), split_axis=1, concat_axis=1, tiled=True)
    grouped = arrived.reshape(local_experts, -1, model_width)
    gate_part = jnp.einsum("erd,edf->erf", grouped, expert_gate, preferred_element_type=jnp.float32)
    up_part = jnp.einsum("erd,edf->erf", grouped, expert_up, preferred_element_type=jnp.float32)
    hidden = (jax.nn.silu(gate_part) * up_part).astype(jnp.bfloat16)
    result = jnp.einsum(
        "erf,efd->erd", hidden, expert_down, preferred_element_type=jnp.float32
    ).astype(jnp.bfloat16)
    returned = lax.all_to_all(
        result.reshape(arrived.shape), ("sp", "tp"), split_axis=1, concat_axis=1, tiled=True
    )
    gathered = jnp.dot(
        placement, returned.reshape(-1, model_width), preferred_element_type=jnp.float32
    )
    weighted = gathered.reshape(row_count, pick_count, model_width) * route_weights[:, :, None]
    return jnp.sum(weighted, axis=1)


def body(
    queries,
    key_heads,
    value_heads,
    head_gain,
    residual,
    out_weight,
    norm_gain,
    shared_gate,
    shared_up,
    shared_down,
    expert_gate,
    expert_up,
    expert_down,
    routed_experts,
    route_weights,
):
    head_output = head_norm(stick_breaking(queries, key_heads, value_heads), head_gain)
    token_heads = lax.all_to_all(head_output, "tp", split_axis=0, concat_axis=1, tiled=True)
    branch = jnp.dot(token_heads, out_weight, preferred_element_type=jnp.float32)
    stream = (residual.astype(jnp.float32) + branch).astype(jnp.bfloat16)
    stream_wide = stream.astype(jnp.float32)
    inverse = lax.rsqrt(jnp.mean(stream_wide * stream_wide, axis=1, keepdims=True) + EPSILON)
    expert_input = (stream_wide * inverse * norm_gain).astype(jnp.bfloat16)
    shared_hidden = (
        jax.nn.silu(jnp.dot(expert_input, shared_gate, preferred_element_type=jnp.float32))
        * jnp.dot(expert_input, shared_up, preferred_element_type=jnp.float32)
    ).astype(jnp.bfloat16)
    shared_term = jnp.dot(shared_hidden, shared_down, preferred_element_type=jnp.float32)
    routed = routed_sum(
        expert_input, expert_gate, expert_up, expert_down, routed_experts, route_weights
    )
    return (stream_wide + shared_term + routed).astype(jnp.bfloat16)


def solution(mesh):
    return jax.shard_map(
        body,
        mesh=mesh,
        in_specs=(
            P("sp", "tp"),
            P("sp", "tp"),
            P("sp", "tp"),
            P("tp"),
            P(("sp", "tp"), None),
            P(),
            P(),
            P(),
            P(),
            P(),
            P(("sp", "tp"), None, None),
            P(("sp", "tp"), None, None),
            P(("sp", "tp"), None, None),
            P(("sp", "tp"), None),
            P(("sp", "tp"), None),
        ),
        out_specs=P(("sp", "tp"), None),
        check_vma=False,
    )
```

profile of v0, /device:TPU:0, one launch (start us, length us, event | category | flops | bytes accessed | tf_op | source)
XLA Modules:
  0.0 514.6 jit_solution(18393780882637082508)
XLA Ops:
  6.5 0.0 all-gather.3.cloned.1.call-start
  6.5 0.7 all-gather.3.cloned.1.call-update
  7.3 0.0 all-gather.5.cloned.1.call-start
  7.3 0.7 all-gather.5.cloned.1.call-update
  8.0 0.8 copy.105
  8.8 0.1 eq.67
  8.9 0.1 eq.63
  9.0 1.7 copy.100
  10.7 1.2 reduce-window.24
  11.9 0.2 slice_reduce_fusion
  12.2 0.1 fusion.48
  12.3 0.1 sub.24
  12.5 0.1 copy.108
  12.5 0.7 fusion.54
  13.2 39.3 %all-gather.3.cloned.1.call-done = bf16[4096,128]{1,0:T(8,128)(2,1)} async-done(((bf16[512,128]{1,0:T(8,128)(2,1)}), bf16[4096,128]{1,0:T(8,128)(2,1)}) %all-gather.3.cloned.1.call-update) | async-done | bytes 1048592 | tf_op jit(solution)/shard_map/all_gather | solution.py:65
  52.5 5.0 reshape.227
  57.5 5.9 %copy.102 = bf16[8,512,2,64]{1,3,2,0:T(8,128)(2,1)} copy(bf16[8,512,2,64]{3,2,1,0:T(2,128)(2,1)} %reshape.227) | data formatting | bytes 2097152 | tf_op jit(solution)/shard_map/while | solution.py:91
  63.3 30.3 %all-gather.5.cloned.1.call-done = bf16[4096,128]{1,0:T(8,128)(2,1)} async-done(((bf16[512,128]{1,0:T(8,128)(2,1)}), bf16[4096,128]{1,0:T(8,128)(2,1)}) %all-gather.5.cloned.1.call-update) | async-done | bytes 1048592 | tf_op jit(solution)/shard_map/all_gather | solution.py:68
  93.6 5.0 reshape.228
  98.6 4.6 copy.103
  103.2 29.2 %while.14 = (s32[]{:T(128)}, f32[8,512,2]{1,2,0:T(2,128)S(1)}, f32[8,512,2,64]{1,3,2,0:T(8,128)}, s32[]{:T(128)}, s32[1]{0:T(128)}, /*index=5*/bf16[8,512,2,64]{...) while((s32[]{:T(128)}, f32[8,512,2]{1,2,0:T(2,128)S(1)}, ...), condition=%wide.region_6.7_spmd, body=%wide.region_0.6_spmd.sunk | while | flops 217857024 | bytes 41952508 | solution.py:91
  103.4 22.4 %conditional.2 = (f32[1,512,2]{1,2,0:T(2,128)S(1)}, f32[1,512,2,64]{1,3,2,0:T(8,128)S(1)}) conditional(s32[]{:T(128)} %convert_element_type.93, () %tuple.56, (s32[]{:T(128)}, s32[1]{0:T(128)}, bf16[8,512,2,64]{1,3,2,0:T(8,128)(2,1)}, bf16[1,512,2,64]{1,3,2,0:T(8,128)(2,1)}, bf16[8,512,2,64]{1,3,2,0:T(8,128)(2,1)S(1)}) %tuple.57), branch_computations={%region_1.1_spmd, %region_2.5_spmd} | conditional | flops 217857024 | bytes 41419364 | solution.py:86
  103.5 0.2 broadcast_compare_fusion
  103.7 4.0 fusion.1
  107.7 9.6 %fusion.11 = f32[2,512,4,128]{1,2,3,0:T(4,128)S(1)} fusion(f32[2,512,4,128]{1,3,2,0:T(8,128)S(1)} %bitcast.90), kind=kOutput, calls=%fused_computation.17 | output fusion | flops 66584576 | bytes 4194304 | tf_op jit(solution)/shard_map/reduce-window.6
  117.3 1.3 copy-done.1
  118.7 2.0 broadcast_add_fusion
  120.7 0.6 copy.97
  121.3 1.0 copy-done.2
  122.2 3.3 fusion.6
  125.6 0.3 convolution_bitcast_fusion
  125.9 0.7 constant_dynamic-update-slice_fusion.5
  126.6 0.7 constant_dynamic-update-slice_fusion.5
  127.4 0.7 constant_dynamic-update-slice_fusion.5
  128.2 0.7 constant_dynamic-update-slice_fusion.5
  129.0 0.7 constant_dynamic-update-slice_fusion.5
  129.8 0.7 constant_dynamic-update-slice_fusion.5
  130.6 0.7 constant_dynamic-update-slice_fusion.5
  131.4 0.7 constant_dynamic-update-slice_fusion.5
  132.5 0.0 copy-start.5
  132.5 1.9 multiply_reduce_fusion.1
  134.5 0.1 mul.121
  134.6 0.2 multiply_convert_fusion.2
  134.8 0.7 copy.104
  135.5 3.5 all-to-all-start
  139.0 0.2 fusion.39
  139.2 4.3 all-to-all-done
  143.5 1.6 multiply_reduce_fusion.2
  145.2 2.7 convolution_convert_fusion.1
  147.9 6.1 %reshape.222 = bf16[2,32,12,2048]{3,2,1,0:T(8,128)(2,1)} reshape(bf16[768,2048]{1,0:T(8,128)(2,1)} %convolution_convert_fusion.1) | data formatting | bytes 6291456 | tf_op jit(solution)/shard_map/reshape | solution.py:120
  154.0 5.5 %copy.109 = bf16[2,32,12,2048]{3,0,2,1:T(2,128)(2,1)S(1)} copy(bf16[2,32,12,2048]{3,2,1,0:T(8,128)(2,1)} %reshape.222) | data formatting | bytes 6291456 | tf_op jit(solution)/shard_map/reshape | solution.py:120
  159.4 0.0 copy-start.6
  159.5 230.0 %all_to_all.26 = bf16[2,32,12,2048]{3,0,2,1:T(2,128)(2,1)S(1)} all-to-all(bf16[2,32,12,2048]{3,0,2,1:T(2,128)(2,1)S(1)} %copy.109), channel_id=1, replica_groups=mesh['sp'=8,'tp'=4] {'sp','tp'}, dimensions={1} | all-to-all | bytes 6291456 | tf_op jit(solution)/shard_map/all_to_all | solution.py:121
  389.4 1.7 copy-done.3
  391.1 3.2 fusion.24
  394.3 10.3 %convolution_convert_fusion = bf16[2,384,2048]{2,1,0:T(8,128)(2,1)} fusion(bf16[2,512,2048]{2,1,0:T(8,128)(2,1)} %param.31, f32[2,384,512]{2,1,0:T(8,128)} %fusion.24, bf16[2,2048,512]{2,1,0:T(8,128)(2,1)} %param.30, bf16[2,384,2048]{2,0,1:T(2,128)(2,1)} %bitcast.93), kind=kOutput, calls=%fused_computation.37 | convolution fusion | flops 3225157632 | bytes 16252928 | tf_op jit(solution)/shard_map/erf,efd->erd/dot_general | solution.py:126
  404.6 6.8 %copy.112 = bf16[2,384,2048]{2,0,1:T(2,128)(2,1)} copy(bf16[2,384,2048]{2,1,0:T(8,128)(2,1)} %convolution_convert_fusion) | data formatting | bytes 6291456 | tf_op jit(solution)/shard_map/convert_element_type | solution.py:128
  411.5 4.0 all-to-all-start.2
  415.4 2.1 fusion.59
  417.5 69.5 %all-to-all-done.2 = bf16[2,32,12,2048]{3,0,2,1:T(2,128)(2,1)} async-done(((bf16[2,32,12,2048]{3,0,2,1:T(2,128)(2,1)}), bf16[2,32,12,2048]{3,0,2,1:T(2,128)(2,1)}, u32[]{:S(2)}, u32[]{:S(2)}) %all-to-all-start.2) | async-done | bytes 3145760 | tf_op jit(solution)/shard_map/all_to_all | solution.py:129
  487.0 5.4 %copy.113 = bf16[2,32,12,2048]{3,2,1,0:T(8,128)(2,1)} copy(bf16[2,32,12,2048]{3,0,2,1:T(2,128)(2,1)} %all-to-all-done.2) | data formatting | bytes 6291456 | tf_op jit(solution)/shard_map/all_to_all | solution.py:129
  492.4 6.2 %reshape.226 = bf16[768,2048,1]{1,0,2:T(8,128)(2,1)} reshape(bf16[2,32,12,2048]{3,2,1,0:T(8,128)(2,1)} %copy.113) | data formatting | bytes 6291456 | tf_op jit(solution)/shard_map/reshape | solution.py:133
  498.6 4.8 multiply_reduce_fusion
  503.4 4.2 fusion.29
  (55 shorter events, 0.7 us)
Async XLA Ops:
  6.5 137.0 %copy-start = (bf16[512,2048]{1,0:T(8,128)(2,1)S(1)}, bf16[512,2048]{1,0:T(8,128)(2,1)}, u32[]{:S(2)}) copy-start(bf16[512,2048]{1,0:T(8,128)(2,1)} %param.24) | copy-start | bytes 6291460
  6.5 46.0 %all-gather.3.cloned.1.call-start = ((), (), s32[]{:S(2)}) async-start(), calls=%async_computation.3 | async-start | bytes 1179648 | tf_op jit(solution)/shard_map/all_gather | solution.py:65
  7.3 86.4 %all-gather.5.cloned.1.call-start = ((), (), s32[]{:S(2)}) async-start(), calls=%async_computation.4 | async-start | bytes 1179648 | tf_op jit(solution)/shard_map/all_gather | solution.py:68
  117.3 1.3 copy-start.1
  120.6 1.6 copy-start.2
  132.5 2.1 copy-start.5
  135.5 9.6 %copy-start.4 = (f32[2048]{0:T(1024)S(1)}, f32[2048]{0:T(1024)}, u32[]{:S(2)}) copy-start(f32[2048]{0:T(1024)} %param.25) | copy-start | bytes 24580
  135.5 8.0 %all-to-all-start = ((bf16[4,128,128]{1,2,0:T(8,128)(2,1)}), bf16[4,128,128]{1,2,0:T(8,128)(2,1)S(1)}, u32[]{:S(2)}, u32[]{:S(2)}) async-start(bf16[4,128,128]{1,2,0:T(8,128)(2,1)} %copy.104), calls=%async_computation | async-start | bytes 262144 | tf_op jit(solution)/shard_map/all_to_all | solution.py:157
  159.4 231.7 %copy-start.6 = (bf16[2,2048,512]{2,1,0:T(8,128)(2,1)S(1)}, bf16[2,2048,512]{2,1,0:T(8,128)(2,1)}, u32[]{:S(2)}) copy-start(bf16[2,2048,512]{2,1,0:T(8,128)(2,1)} %param.29) | copy-start | bytes 12582916
  389.4 1.7 copy-start.3
  411.5 75.5 %all-to-all-start.2 = ((bf16[2,32,12,2048]{3,0,2,1:T(2,128)(2,1)}), bf16[2,32,12,2048]{3,0,2,1:T(2,128)(2,1)}, u32[]{:S(2)}, u32[]{:S(2)}) async-start(bf16[2,32,12,2048]{3,0,2,1:T(2,128)(2,1)} %bitcast.91), calls=%async_computation.2 | async-start | bytes 6291456 | tf_op jit(solution)/shard_map/all_to_all | solution.py:129
  492.4 6.2 %copy-start.7 = (f32[128,4]{0,1:T(4,128)S(1)}, f32[128,4]{0,1:T(4,128)}, u32[]{:S(2)}) copy-start(f32[128,4]{0,1:T(4,128)} %param.33) | copy-start | bytes 6148
Sparse Core Ops, SparseCore 0:
  9.5 42.9 all-gather.2
  54.6 38.9 all-gather.4
where the time goes:
time: 520 us; the launch traced here: 515 us
  blocking collectives  230 us (44%)
  waiting for transfers between devices  145 us (28%)
  local copies, waits for them, and re-layouts  64.9 us (12%)
  matrix products  33.1 us (6%)
  other arithmetic  19.7 us (4%)
  between operations  13.8 us (3%)
  starting transfers between devices  7.45 us (1%)
    all_to_all x1, blocking collectives, routed_sum(): lax.all_to_all(outgoing, ('sp', 'tp'), split_axis=1, concat_axis=1, tiled...  230 us
    all_to_all x1, waiting for transfers between devices, routed_sum(): lax.all_to_all(result.reshape(arrived.shape), ('sp', 'tp'), split_axis=1,...  69.5 us
    all_gather x1, waiting for transfers between devices, stick_breaking(): lax.all_gather(key_heads, 'sp', axis=0, tiled=True)  39.3 us
    all_gather x1, waiting for transfers between devices, stick_breaking(): lax.all_gather(value_heads, 'sp', axis=0, tiled=True)  30.3 us
    reshape x2, local copies, waits for them, and re-layouts, routed_sum(): outgoing.reshape(local_experts, device_count, capacity, model_width)  11.5 us
    another operation x4, other arithmetic  10.9 us
    while x2, local copies, waits for them, and re-layouts, stick_breaking(): totals, partials = lax.fori_loop(0, key_piece.shape[0], add_one, initial)  10.5 us
  transfers between devices with their start and end apart: 4, of which 4 were waited for; matrix products, arithmetic and copies ran while one was open for 4% of the time, Pallas kernels for 0%

commit v1 on v0

--- a/solution.py
+++ b/solution.py
@@ -6,6 +6,19 @@
 
 HEAD_DIM = 64
 EPSILON = 1e-06
+
+
+def _cover_records(frame):
+    now = jnp.concatenate(
+        lax.all_to_all(
+            jnp.stack(jnp.split(frame, lax.axis_size(("sp", "tp")), axis=1), axis=0),
+            ("sp", "tp"),
+            0,
+            0,
+        ),
+        axis=1,
+    )
+    return now
 
 
 def block_terms(query_block, key_block, value_block, query_start, key_start):
@@ -126,9 +139,7 @@
     result = jnp.einsum(
         "erf,efd->erd", hidden, expert_down, preferred_element_type=jnp.float32
     ).astype(jnp.bfloat16)
-    returned = lax.all_to_all(
-        result.reshape(arrived.shape), ("sp", "tp"), split_axis=1, concat_axis=1, tiled=True
-    )
+    returned = _cover_records(result.reshape(arrived.shape))
     gathered = jnp.dot(
         placement, returned.reshape(-1, model_width), preferred_element_type=jnp.float32
     )

time: 520 us -> 539 us (1.037)
  local copies, waits for them, and re-layouts: 64.9 us -> 85.6 us
    unnamed x14 -> x49, local copies, waits for them, and re-layouts: 4.18 us -> 25.9 us
    another operation x4 -> x6, local copies, waits for them, and re-layouts: 0.25 us -> 7.12 us  [the longest x1 6.17 us: routed_sum(): returned.reshape(-1, model_width)]
    all_to_all x1 -> x0, local copies, waits for them, and re-layouts: 5.41 us -> none  [routed_sum(): lax.all_to_all(result.reshape(arrived.shape), ('sp', 'tp'), split_axis=1,...]
  transfers between devices with their start and end apart: 4 -> 4, of which waited for: 4 -> 4; matrix products, arithmetic and copies ran while one was open for 4% -> 3% of each run, Pallas kernels for 0% -> 0%
where the time goes in v1:
time: 539 us; the launch traced here: 534 us
  blocking collectives  230 us (43%)
  waiting for transfers between devices  146 us (27%)
  local copies, waits for them, and re-layouts  85.6 us (16%)
  matrix products  30.1 us (6%)
  other arithmetic  19.7 us (4%)
  between operations  13.8 us (3%)
  starting transfers between devices  7.4 us (1%)
    all_to_all x1, blocking collectives, routed_sum(): lax.all_to_all(outgoing, ('sp', 'tp'), split_axis=1, concat_axis=1, tiled...  230 us
    all_to_all x1, waiting for transfers between devices, _cover_records(): lax.all_to_all(jnp.stack(jnp.split(frame, lax.axis_size(('sp', 'tp')), ax...  71.1 us
    all_gather x1, waiting for transfers between devices, stick_breaking(): lax.all_gather(key_heads, 'sp', axis=0, tiled=True)  39.3 us
    all_gather x1, waiting for transfers between devices, stick_breaking(): lax.all_gather(value_heads, 'sp', axis=0, tiled=True)  30.3 us
    unnamed x49, local copies, waits for them, and re-layouts  25.9 us
    reshape x2, local copies, waits for them, and re-layouts, routed_sum(): outgoing.reshape(local_experts, device_count, capacity, model_width)  11.5 us
    another operation x4, other arithmetic  10.9 us
  transfers between devices with their start and end apart: 4, of which 4 were waited for; matrix products, arithmetic and copies ran while one was open for 3% of the time, Pallas kernels for 0%

profile of v1, /device:TPU:0, one launch (start us, length us, event | category | flops | bytes accessed | tf_op | source)
XLA Modules:
  0.0 533.8 jit_solution(12415297107952839414)
XLA Ops:
  6.5 0.7 all-gather.3.cloned.1.call-update
  8.0 0.8 copy.137
  9.0 1.7 copy.132
  10.7 1.2 reduce-window.24
  12.5 0.7 fusion.86
  13.2 39.3 %all-gather.3.cloned.1.call-done = bf16[4096,128]{1,0:T(8,128)(2,1)} async-done(((bf16[512,128]{1,0:T(8,128)(2,1)}), bf16[4096,128]{1,0:T(8,128)(2,1)}) %all-gather.3.cloned.1.call-update) | async-done | bytes 1048592 | tf_op jit(solution)/shard_map/all_gather | solution.py:78
  52.5 5.0 reshape.227
  57.5 5.9 %copy.134 = bf16[8,512,2,64]{1,3,2,0:T(8,128)(2,1)} copy(bf16[8,512,2,64]{3,2,1,0:T(2,128)(2,1)} %reshape.227) | data formatting | bytes 2097152 | tf_op jit(solution)/shard_map/while | solution.py:104
  63.3 30.3 %all-gather.5.cloned.1.call-done = bf16[4096,128]{1,0:T(8,128)(2,1)} async-done(((bf16[512,128]{1,0:T(8,128)(2,1)}), bf16[4096,128]{1,0:T(8,128)(2,1)}) %all-gather.5.cloned.1.call-update) | async-done | bytes 1048592 | tf_op jit(solution)/shard_map/all_gather | solution.py:81
  93.6 5.0 reshape.228
  98.6 4.6 copy.135
  103.2 29.2 %while.14 = (s32[]{:T(128)}, f32[8,512,2]{1,2,0:T(2,128)S(1)}, f32[8,512,2,64]{1,3,2,0:T(8,128)}, s32[]{:T(128)}, s32[1]{0:T(128)}, /*index=5*/bf16[8,512,2,64]{...) while((s32[]{:T(128)}, f32[8,512,2]{1,2,0:T(2,128)S(1)}, ...), condition=%wide.region_6.7_spmd, body=%wide.region_0.6_spmd.sunk | while | flops 217857024 | bytes 41952508 | solution.py:104
  103.4 22.4 %conditional.2 = (f32[1,512,2]{1,2,0:T(2,128)S(1)}, f32[1,512,2,64]{1,3,2,0:T(8,128)S(1)}) conditional(s32[]{:T(128)} %convert_element_type.93, () %tuple.56, (s32[]{:T(128)}, s32[1]{0:T(128)}, bf16[8,512,2,64]{1,3,2,0:T(8,128)(2,1)}, bf16[1,512,2,64]{1,3,2,0:T(8,128)(2,1)}, bf16[8,512,2,64]{1,3,2,0:T(8,128)(2,1)S(1)}) %tuple.57), branch_computations={%region_1.1_spmd, %region_2.5_spmd} | conditional | flops 217857024 | bytes 41419364 | solution.py:99
  103.7 4.0 fusion.1
  107.7 9.6 %fusion.11 = f32[2,512,4,128]{1,2,3,0:T(4,128)S(1)} fusion(f32[2,512,4,128]{1,3,2,0:T(8,128)S(1)} %bitcast.221), kind=kOutput, calls=%fused_computation.17 | output fusion | flops 66584576 | bytes 4194304 | tf_op jit(solution)/shard_map/reduce-window.6
  117.3 1.3 copy-done.2
  118.7 2.0 broadcast_add_fusion
  121.3 1.0 copy-done.3
  122.2 3.3 fusion.6
  125.9 0.7 constant_dynamic-update-slice_fusion.5
  126.6 0.7 constant_dynamic-update-slice_fusion.5
  127.4 0.7 constant_dynamic-update-slice_fusion.5
  128.2 0.7 constant_dynamic-update-slice_fusion.5
  129.0 0.7 constant_dynamic-update-slice_fusion.5
  129.8 0.7 constant_dynamic-update-slice_fusion.5
  130.6 0.7 constant_dynamic-update-slice_fusion.5
  131.4 0.7 constant_dynamic-update-slice_fusion.5
  132.5 1.9 multiply_reduce_fusion.1
  135.5 3.3 all-to-all-start
  139.1 4.3 all-to-all-done
  143.4 1.6 multiply_reduce_fusion.2
  145.0 2.7 convolution_convert_fusion.1
  147.8 6.1 %reshape.222 = bf16[2,32,12,2048]{3,2,1,0:T(8,128)(2,1)} reshape(bf16[768,2048]{1,0:T(8,128)(2,1)} %convolution_convert_fusion.1) | data formatting | bytes 6291456 | tf_op jit(solution)/shard_map/reshape | solution.py:133
  153.8 5.5 %copy.141 = bf16[2,32,12,2048]{3,0,2,1:T(2,128)(2,1)S(1)} copy(bf16[2,32,12,2048]{3,2,1,0:T(8,128)(2,1)} %reshape.222) | data formatting | bytes 6291456 | tf_op jit(solution)/shard_map/reshape | solution.py:133
  159.3 230.0 %all_to_all.26 = bf16[2,32,12,2048]{3,0,2,1:T(2,128)(2,1)S(1)} all-to-all(bf16[2,32,12,2048]{3,0,2,1:T(2,128)(2,1)S(1)} %copy.141), channel_id=1, replica_groups=mesh['sp'=8,'tp'=4] {'sp','tp'}, dimensions={1} | all-to-all | bytes 6291456 | tf_op jit(solution)/shard_map/all_to_all | solution.py:134
  389.3 1.7 copy-done.4
  391.0 2.0 fusion.24
  393.0 9.9 %convolution_convert_fusion = bf16[2,384,2048]{2,1,0:T(8,128)(2,1)} fusion(bf16[2,512,2048]{2,1,0:T(8,128)(2,1)} %param.31, f32[2,384,512]{2,1,0:T(8,128)S(1)} %fusion.24, bf16[2,2048,512]{2,1,0:T(8,128)(2,1)} %param.30, bf16[2,384,2048]{2,0,1:T(2,128)(2,1)} %bitcast.255), kind=kOutput, calls=%fused_computation.37 | convolution fusion | flops 3225157632 | bytes 16252928 | tf_op jit(solution)/shard_map/erf,efd->erd/dot_general | solution.py:139
  402.9 5.1 copy.144
  408.7 0.7 fusion.81
  409.4 0.7 fusion.80
  410.1 0.7 fusion.79
  410.8 0.7 fusion.78
  412.2 0.7 fusion.76
  413.6 0.7 fusion.74
  415.0 0.7 fusion.72
  416.4 0.7 fusion.70
  417.8 0.7 fusion.68
  418.6 0.7 fusion.67
  420.7 0.7 fusion.64
  422.1 0.7 fusion.62
  422.8 0.7 fusion.61
  424.2 0.7 fusion.59
  424.9 0.7 fusion.58
  426.3 0.7 fusion.56
  427.7 0.7 fusion.54
  429.1 0.7 fusion.52
  429.8 0.7 fusion.51
  430.5 4.0 all-to-all-start.2
  435.0 71.1 %all-to-all-done.2 = bf16[32,2,1,12,2048]{4,1,3,2,0:T(2,128)(2,1)} async-done(((bf16[32,2,1,12,2048]{4,1,3,2,0:T(2,128)(2,1)}), bf16[32,2,1,12,2048]{4,1,3,2,0:T(2,128)(2,1)}, u32[]{:S(2)}, u32[]{:S(2)}) %all-to-all-start.2) | async-done | bytes 3145760 | tf_op jit(solution)/shard_map/all_to_all | solution.py:13
  506.1 5.4 %copy.145 = bf16[2,32,1,12,2048]{4,3,1,0,2:T(8,128)(2,1)} copy(bf16[2,32,1,12,2048]{4,0,3,2,1:T(2,128)(2,1)} %bitcast.52) | data formatting | bytes 6291456 | tf_op jit(solution)/shard_map/reshape | solution.py:12
  511.5 6.2 %reshape.226 = bf16[768,2048,1]{1,0,2:T(8,128)(2,1)} reshape(bf16[2,32,1,12,2048]{4,3,1,0,2:T(8,128)(2,1)} %copy.145) | data formatting | bytes 6291456 | tf_op jit(solution)/shard_map/reshape;reshape | solution.py:144
  517.7 4.9 multiply_reduce_fusion
  522.6 4.2 fusion.29
  (91 shorter events, 14.1 us)
Async XLA Ops:
  6.5 136.9 %copy-start = (bf16[512,2048]{1,0:T(8,128)(2,1)S(1)}, bf16[512,2048]{1,0:T(8,128)(2,1)}, u32[]{:S(2)}) copy-start(bf16[512,2048]{1,0:T(8,128)(2,1)} %param.24) | copy-start | bytes 6291460
  6.5 46.0 %all-gather.3.cloned.1.call-start = ((), (), s32[]{:S(2)}) async-start(), calls=%async_computation.3 | async-start | bytes 1179648 | tf_op jit(solution)/shard_map/all_gather | solution.py:78
  7.3 86.4 %all-gather.5.cloned.1.call-start = ((), (), s32[]{:S(2)}) async-start(), calls=%async_computation.4 | async-start | bytes 1179648 | tf_op jit(solution)/shard_map/all_gather | solution.py:81
  117.3 1.3 copy-start.2
  120.6 1.6 copy-start.3
  132.5 2.1 copy-start.7
  134.4 10.6 %copy-start.6 = (f32[2048]{0:T(1024)S(1)}, f32[2048]{0:T(1024)}, u32[]{:S(2)}) copy-start(f32[2048]{0:T(1024)} %param.25) | copy-start | bytes 24580
  135.5 7.9 %all-to-all-start = ((bf16[4,128,128]{1,2,0:T(8,128)(2,1)}), bf16[4,128,128]{1,2,0:T(8,128)(2,1)S(1)}, u32[]{:S(2)}, u32[]{:S(2)}) async-start(bf16[4,128,128]{1,2,0:T(8,128)(2,1)} %copy.136), calls=%async_computation | async-start | bytes 262144 | tf_op jit(solution)/shard_map/all_to_all | solution.py:168
  159.3 231.7 %copy-start.8 = (bf16[2,2048,512]{2,1,0:T(8,128)(2,1)S(1)}, bf16[2,2048,512]{2,1,0:T(8,128)(2,1)}, u32[]{:S(2)}) copy-start(bf16[2,2048,512]{2,1,0:T(8,128)(2,1)} %param.29) | copy-start | bytes 12582916
  389.3 1.7 copy-start.4
  430.5 4.0 copy-start.5
  430.5 75.6 %all-to-all-start.2 = ((bf16[32,2,1,12,2048]{4,1,3,2,0:T(2,128)(2,1)}), bf16[32,2,1,12,2048]{4,1,3,2,0:T(2,128)(2,1)}, u32[]{:S(2)}, u32[]{:S(2)}) async-start(bf16[32,2,1,12,2048]{4,1,3,2,0:T(2,128)(2,1)} %fusion.51), calls=%async_computation.2 | async-start | bytes 6291456 | tf_op jit(solution)/shard_map/all_to_all | solution.py:13
  511.5 6.2 %copy-start.9 = (f32[128,4]{0,1:T(4,128)S(1)}, f32[128,4]{0,1:T(4,128)}, u32[]{:S(2)}) copy-start(f32[128,4]{0,1:T(4,128)} %param.33) | copy-start | bytes 6148
  517.7 9.1 %copy-start.1 = (bf16[512,2048]{1,0:T(8,128)(2,1)S(1)}, bf16[512,2048]{1,0:T(8,128)(2,1)}, u32[]{:S(2)}) copy-start(bf16[512,2048]{1,0:T(8,128)(2,1)} %param.24) | copy-start | bytes 6291460
Sparse Core Ops, SparseCore 0:
  9.5 42.9 all-gather.2
  54.6 38.9 all-gather.4
